TPU v7x, 32 devices: a whole 2x2x4 slice. The times are simulated.
32 devices in a mesh: fs: 8 (over z, y), tp: 4 (over x, core).
Axes of the slice: x: 2, y: 2, z: 4, core: 2. Of those that a mesh axis runs over, the one named last changes fastest.
Arguments:
- tokens: bfloat16 [8192, 2048], P('fs', 'tp'), may hold values from -6 to 6
- norm_gain: float32 [2048], P('fs'), may hold values from 0.1 to 1.9
- up_master: float32 [2048, 4096], P('fs', 'tp'), may hold values from -0.125 to 0.125
- down_master: float32 [4096, 2048], P('fs', 'tp'), may hold values from -0.09375 to 0.09375
Outputs:
- mixed: bfloat16 [8192, 2048], P('fs', 'tp')
- up_ready: bfloat16 [2048, 4096], P(None, 'tp')
- down_ready: bfloat16 [4096, 2048], P('tp')
All inputs are finite; a program needn't handle non-finite values.
Results may differ from a plain program's by a relative error of at most 0.0095.
Values may be sent and summed in bfloat16 or wider, within the bound.
A program may use at most 128 MiB of HBM per device.

v0:
```python
import jax
import jax.numpy as jnp
from jax import lax
from jax.sharding import PartitionSpec as P


def shards(tokens, norm_gain, up_master, down_master):
    up_local = (norm_gain[:, None] * up_master).astype(jnp.bfloat16)
    up_ready = lax.all_gather(up_local, "fs", axis=0, tiled=True)
    down_local = down_master.astype(jnp.bfloat16)
    gathered = lax.all_gather(down_local, "fs", axis=0, tiled=True)
    down_ready = lax.all_to_all(gathered, "tp", split_axis=0, concat_axis=1, tiled=True)
    features = lax.all_gather(tokens, "tp", axis=1, tiled=True)
    values = features.astype(jnp.float32)
    mean_square = jnp.mean(values * values, axis=-1, keepdims=True)
    normed = (values * lax.rsqrt(mean_square + 1e-06)).astype(jnp.bfloat16)
    before = jnp.dot(normed, up_ready, preferred_element_type=jnp.float32)
    hidden = jnp.square(jax.nn.relu(before)).astype(jnp.bfloat16)
    partial_value = jnp.dot(hidden, down_ready, preferred_element_type=jnp.float32)
    mixed = lax.psum_scatter(
        partial_value.astype(jnp.bfloat16), "tp", scatter_dimension=1, tiled=True
    )
    return (mixed, up_ready, down_ready)


def solution(mesh):
    return jax.shard_map(
        shards,
        mesh=mesh,
        in_specs=(P("fs", "tp"), P("fs"), P("fs", "tp"), P("fs", "tp")),
        out_specs=(P("fs", "tp"), P(None, "tp"), P("tp", None)),
        check_vma=False,
    )
```

profile of v0, /device:TPU:0, one launch (start us, length us, event | category | flops | bytes accessed | tf_op | source)
XLA Modules:
  0.0 287.9 jit_solution(17428654618168584598)
XLA Ops:
  7.2 0.0 all-gather.8.cloned.1.call-start
  7.2 2.1 convert_element_type.22
  9.3 0.0 all-gather.8.cloned.1.call-update
  9.3 0.0 all-gather.4.cloned.1.call-start
  9.4 0.7 all-gather.4.cloned.1.call-update
  10.1 0.0 all-gather.6.cloned.1.call-start
  10.1 2.1 multiply_convert_fusion.2
  12.3 0.0 all-gather.6.cloned.1.call-update
  12.3 73.9 %all-gather.8.cloned.1.call-done = bf16[4096,512]{1,0:T(8,128)(2,1)} async-done(((bf16[512,512]{1,0:T(8,128)(2,1)}), bf16[4096,512]{1,0:T(8,128)(2,1)}) %all-gather.8.cloned.1.call-update) | async-done | bytes 4194320 | tf_op jit(solution)/shard_map/all_gather | solution.py:11
  86.2 4.9 %all-to-all-start = ((bf16[4,1024,512]{2,1,0:T(8,128)(2,1)}), bf16[4,1024,512]{2,1,0:T(8,128)(2,1)}, u32[]{:S(2)}, u32[]{:S(2)}) async-start(bf16[4,1024,512]{2,1,0:T(8,128)(2,1)} %bitcast.8), calls=%async_computation | async-start | bytes 8388608 | tf_op jit(solution)/shard_map/all_to_all | solution.py:12
  91.1 0.0 reduce-scatter.2.cloned.1.call-start
  91.2 52.2 %all-gather.4.cloned.1.call-done = bf16[1024,2048]{1,0:T(8,128)(2,1)} async-done(((bf16[1024,512]{1,0:T(8,128)(2,1)}), bf16[1024,2048]{1,0:T(8,128)(2,1)}) %all-gather.4.cloned.1.call-update) | async-done | bytes 4194320 | tf_op jit(solution)/shard_map/all_gather | solution.py:13
  143.4 3.1 %fusion = f32[1024]{0:T(1024)S(1)} fusion(bf16[1024,2048]{1,0:T(8,128)(2,1)} %all-gather.4.cloned.1.call-done), kind=kLoop, calls=%fused_computation.2 | loop fusion | flops 6290432 | bytes 4198400 | tf_op jit(solution)/shard_map/reduce_sum | solution.py:15
  146.5 15.3 %all-to-all-done = bf16[4,1024,512]{2,1,0:T(8,128)(2,1)} async-done(((bf16[4,1024,512]{2,1,0:T(8,128)(2,1)}), bf16[4,1024,512]{2,1,0:T(8,128)(2,1)}, u32[]{:S(2)}, u32[]{:S(2)}) %all-to-all-start) | async-done | bytes 4194336 | tf_op jit(solution)/shard_map/all_to_all | solution.py:12
  161.8 6.2 %copy.8 = bf16[4,1024,512]{1,2,0:T(8,128)(2,1)} copy(bf16[4,1024,512]{2,1,0:T(8,128)(2,1)} %all-to-all-done) | data formatting | bytes 8388608 | tf_op jit(solution)/shard_map/all_to_all | solution.py:12
  168.0 50.9 %all-gather.6.cloned.1.call-done = bf16[2048,1024]{1,0:T(8,128)(2,1)} async-done(((bf16[256,1024]{1,0:T(8,128)(2,1)}), bf16[2048,1024]{1,0:T(8,128)(2,1)}) %all-gather.6.cloned.1.call-update) | async-done | bytes 4194320 | tf_op jit(solution)/shard_map/all_gather | solution.py:9
  218.9 14.7 %convolution_convert_fusion = bf16[1024,2048]{1,0:T(8,128)(2,1)} fusion(bf16[1024,2048]{0,1:T(8,128)(2,1)} %bitcast.6, bf16[2048,1024]{1,0:T(8,128)(2,1)} %all-gather.6.cloned.1.call-done, bf16[1024,2048]{1,0:T(8,128)(2,1)} %all-gather.4.cloned.1.call-done, f32[1024]{0:T(1024)S(1)} %add_rsqrt_fusion), kind=kOutput, calls=%fused_computation.7 | convolution fusion | flops 8601468928 | bytes 16781312 | tf_op jit(solution)/shard_map/dot_general | solution.py:19
  233.6 0.0 reduce-scatter.2.cloned.1.call-update
  233.6 6.5 %copy.9 = bf16[1024,2048]{1,0:T(8,128)(2,1)} copy(bf16[1024,2048]{0,1:T(8,128)(2,1)} %bitcast.7) | data formatting | bytes 8388608
  240.1 36.6 %reduce-scatter.2.cloned.1.call-done = bf16[1024,512]{1,0:T(8,128)(2,1)} async-done(((bf16[1024,2048]{1,0:T(8,128)(2,1)}), bf16[1024,512]{1,0:T(8,128)(2,1)}) %reduce-scatter.2.cloned.1.call-update) | async-done | bytes 1048592 | tf_op jit(solution)/shard_map/reduce_scatter | solution.py:20
  276.7 4.6 %copy.11 = bf16[2048,1024]{1,0:T(8,128)(2,1)} copy(bf16[2048,1024]{1,0:T(8,128)(2,1)} %all-gather.6.cloned.1.call-done) | data formatting | bytes 8388608
  (1 shorter events, 0.0 us)
Async XLA Ops:
  7.2 79.1 %all-gather.8.cloned.1.call-start = ((), (), s32[]{:S(2)}) async-start(), calls=%async_computation.4 | async-start | bytes 4718592 | tf_op jit(solution)/shard_map/all_gather | solution.py:11
  9.3 134.1 %all-gather.4.cloned.1.call-start = ((), (), s32[]{:S(2)}) async-start(), calls=%async_computation.2 | async-start | bytes 5242880 | tf_op jit(solution)/shard_map/all_gather | solution.py:13
  10.1 208.8 %all-gather.6.cloned.1.call-start = ((), (), s32[]{:S(2)}) async-start(), calls=%async_computation.3 | async-start | bytes 4718592 | tf_op jit(solution)/shard_map/all_gather | solution.py:9
  86.2 75.6 %all-to-all-start = ((bf16[4,1024,512]{2,1,0:T(8,128)(2,1)}), bf16[4,1024,512]{2,1,0:T(8,128)(2,1)}, u32[]{:S(2)}, u32[]{:S(2)}) async-start(bf16[4,1024,512]{2,1,0:T(8,128)(2,1)} %bitcast.8), calls=%async_computation | async-start | bytes 8388608 | tf_op jit(solution)/shard_map/all_to_all | solution.py:12
  91.1 185.6 %reduce-scatter.2.cloned.1.call-start = ((), (), s32[]{:S(2)}) async-start(), calls=%async_computation.5 | async-start | bytes 5242880 | tf_op jit(solution)/shard_map/reduce_scatter | solution.py:20
Sparse Core Ops, SparseCore 0:
  10.7 75.5 all-gather.7
  87.8 55.5 all-gather.3
  146.1 72.7 all-gather.5
  233.7 42.9 reduce-scatter.1
where the time goes:
time: 288 us
  waiting for transfers between devices  230 us (80%)
  local copies, waits for them, and re-layouts  17.3 us (6%)
  matrix products  14.7 us (5%)
  between operations  13.8 us (5%)
  other arithmetic  7.31 us (3%)
  starting transfers between devices  5.06 us (2%)
    all_gather x1, waiting for transfers between devices, shards(): gathered = lax.all_gather(down_local, 'fs', axis=0, tiled=True)  73.9 us
    all_gather x1, waiting for transfers between devices, shards(): features = lax.all_gather(tokens, 'tp', axis=1, tiled=True)  52.2 us
    all_gather x1, waiting for transfers between devices, shards(): up_ready = lax.all_gather(up_local, 'fs', axis=0, tiled=True)  50.9 us
    reduce_scatter x1, waiting for transfers between devices, shards(): lax.psum_scatter(partial_value.astype(jnp.bfloat16), 'tp', scatter_dimens...  36.6 us
    all_to_all x1, waiting for transfers between devices, shards(): lax.all_to_all(gathered, 'tp', split_axis=0, concat_axis=1, tiled=True)  15.3 us
    dot_general x1, matrix products, shards(): jnp.dot(hidden, down_ready, preferred_element_type=jnp.float32)  14.7 us
    unnamed x2, local copies, waits for them, and re-layouts  11.1 us
    all_to_all x1, local copies, waits for them, and re-layouts, shards(): lax.all_to_all(gathered, 'tp', split_axis=0, concat_axis=1, tiled=True)  6.21 us
  transfers between devices with their start and end apart: 5, of which 5 were waited for; matrix products, arithmetic and copies ran while one was open for 6% of the time, Pallas kernels for 0%

commit v1 on v0

--- a/solution.py
+++ b/solution.py
@@ -10,7 +10,8 @@
     down_local = down_master.astype(jnp.bfloat16)
     gathered = lax.all_gather(down_local, "fs", axis=0, tiled=True)
     down_ready = lax.all_to_all(gathered, "tp", split_axis=0, concat_axis=1, tiled=True)
-    features = lax.all_gather(tokens, "tp", axis=1, tiled=True)
+    all_values = lax.all_gather(tokens, "tp")
+    features = jnp.concatenate(all_values, axis=1)
     values = features.astype(jnp.float32)
     mean_square = jnp.mean(values * values, axis=-1, keepdims=True)
     normed = (values * lax.rsqrt(mean_square + 1e-06)).astype(jnp.bfloat16)

time: 288 us -> 288 us (level)
  waiting for transfers between devices: 230 us -> 207 us
  other arithmetic: 7.31 us -> 20.7 us
  local copies, waits for them, and re-layouts: 17.3 us -> 26.1 us
    all_to_all x1, waiting for transfers between devices: 15.3 us -> 0.01 us  [shards(): lax.all_to_all(gathered, 'tp', split_axis=0, concat_axis=1, tiled=True)]
    convert_element_type x0 -> x2, other arithmetic: none -> 13.3 us  [the longest x1 6.71 us: shards(): normed = (values * lax.rsqrt(mean_square + 1e-06)).astype(jnp.bfloat16)]
    convert_element_type x0 -> x1, local copies, waits for them, and re-layouts: none -> 8.81 us  [shards(): values = features.astype(jnp.float32)]
    all_gather x1, waiting for transfers between devices: 50.9 us -> 43.5 us  [shards(): up_ready = lax.all_gather(up_local, 'fs', axis=0, tiled=True)]
  transfers between devices with their start and end apart: 5 -> 5, of which waited for: 5 -> 4; matrix products, arithmetic and copies ran while one was open for 6% -> 14% of each run, Pallas kernels for 0% -> 0%
where the time goes in v1:
time: 288 us; the launch traced here: 287 us
  waiting for transfers between devices  207 us (72%)
  local copies, waits for them, and re-layouts  26.1 us (9%)
  other arithmetic  20.7 us (7%)
  matrix products  14.4 us (5%)
  between operations  13.8 us (5%)
  starting transfers between devices  5.09 us (2%)
    all_gather x1, waiting for transfers between devices, shards(): gathered = lax.all_gather(down_local, 'fs', axis=0, tiled=True)  73.9 us
    all_gather x1, waiting for transfers between devices, shards(): all_values = lax.all_gather(tokens, 'tp')  52.2 us
    all_gather x1, waiting for transfers between devices, shards(): up_ready = lax.all_gather(up_local, 'fs', axis=0, tiled=True)  43.5 us
    reduce_scatter x1, waiting for transfers between devices, shards(): lax.psum_scatter(partial_value.astype(jnp.bfloat16), 'tp', scatter_dimens...  36.7 us
    dot_general x1, matrix products, shards(): jnp.dot(hidden, down_ready, preferred_element_type=jnp.float32)  14.4 us
    unnamed x2, local copies, waits for them, and re-layouts  11.1 us
    convert_element_type x1, local copies, waits for them, and re-layouts, shards(): values = features.astype(jnp.float32)  8.81 us
    convert_element_type x1, other arithmetic, shards(): normed = (values * lax.rsqrt(mean_square + 1e-06)).astype(jnp.bfloat16)  6.71 us
  transfers between devices with their start and end apart: 5, of which 4 were waited for; matrix products, arithmetic and copies ran while one was open for 14% of the time, Pallas kernels for 0%

profile of v1, /device:TPU:0, one launch (start us, length us, event | category | flops | bytes accessed | tf_op | source)
XLA Modules:
  0.0 287.0 jit_solution(16237834668280082924)
XLA Ops:
  7.2 0.0 all-gather.7.cloned.1.call-start
  7.2 2.1 convert_element_type.35
  9.3 0.0 all-gather.7.cloned.1.call-update
  9.3 0.0 all-gather.9.cloned.1.call-start
  9.4 0.7 all-gather.9.cloned.1.call-update
  10.1 0.0 all-gather.5.cloned.1.call-start
  10.1 2.2 multiply_convert_fusion.1
  12.3 0.0 all-gather.5.cloned.1.call-update
  12.3 73.9 %all-gather.7.cloned.1.call-done = bf16[4096,512]{1,0:T(8,128)(2,1)} async-done(((bf16[512,512]{1,0:T(8,128)(2,1)}), bf16[4096,512]{1,0:T(8,128)(2,1)}) %all-gather.7.cloned.1.call-update) | async-done | bytes 4194320 | tf_op jit(solution)/shard_map/all_gather | solution.py:11
  86.2 4.9 %all-to-all-start = ((bf16[4,1024,512]{2,1,0:T(8,128)(2,1)}), bf16[4,1024,512]{2,1,0:T(8,128)(2,1)}, u32[]{:S(2)}, u32[]{:S(2)}) async-start(bf16[4,1024,512]{2,1,0:T(8,128)(2,1)} %bitcast.19), calls=%async_computation | async-start | bytes 8388608 | tf_op jit(solution)/shard_map/all_to_all | solution.py:12
  91.2 0.0 reduce-scatter.2.cloned.1.call-start
  91.2 52.2 %all-gather.9.cloned.1.call-done = bf16[4096,512]{1,0:T(8,128)(2,1)} async-done(((bf16[1024,512]{1,0:T(8,128)(2,1)}), bf16[4096,512]{1,0:T(8,128)(2,1)}) %all-gather.9.cloned.1.call-update) | async-done | bytes 4194320 | tf_op jit(solution)/shard_map/all_gather | solution.py:13
  143.4 6.6 %convert_bitcast_fusion = f32[1024,4,512]{2,0,1:T(8,128)} fusion(bf16[4096,512]{1,0:T(8,128)(2,1)} %all-gather.9.cloned.1.call-done), kind=kLoop, calls=%fused_computation.1 | loop fusion | flops 2097152 | bytes 12582912 | tf_op jit(solution)/shard_map/convert_element_type | solution.py:15
  150.0 8.8 %copy.12 = f32[1024,4,512]{0,2,1:T(8,128)} copy(f32[1024,4,512]{2,0,1:T(8,128)} %convert_bitcast_fusion) | data formatting | bytes 16777216 | tf_op jit(solution)/shard_map/convert_element_type | solution.py:15
  158.8 3.1 %fusion = f32[1024]{0:T(1024)S(1)} fusion(bf16[4,1024,512]{2,1,0:T(8,128)(2,1)} %bitcast.16), kind=kLoop, calls=%fused_computation.2 | loop fusion | flops 6290432 | bytes 4198400 | tf_op jit(solution)/shard_map/reduce_sum | solution.py:16
  161.9 6.7 %fusion.1 = bf16[1024,2048]{0,1:T(8,128)(2,1)} fusion(f32[1024,4,512]{0,2,1:T(8,128)} %copy.12, f32[1024]{0:T(1024)S(1)} %add_rsqrt_fusion), kind=kLoop, calls=%fused_computation.4 | loop fusion | flops 4194304 | bytes 12587008 | tf_op jit(solution)/shard_map/convert_element_type | solution.py:17
  168.6 0.0 all-to-all-done
  168.6 6.2 %copy.13 = bf16[4,1024,512]{1,2,0:T(8,128)(2,1)} copy(bf16[4,1024,512]{2,1,0:T(8,128)(2,1)} %all-to-all-done) | data formatting | bytes 8388608 | tf_op jit(solution)/shard_map/all_to_all | solution.py:12
  174.8 43.5 %all-gather.5.cloned.1.call-done = bf16[2048,1024]{1,0:T(8,128)(2,1)} async-done(((bf16[256,1024]{1,0:T(8,128)(2,1)}), bf16[2048,1024]{1,0:T(8,128)(2,1)}) %all-gather.5.cloned.1.call-update) | async-done | bytes 4194320 | tf_op jit(solution)/shard_map/all_gather | solution.py:9
  218.3 14.4 %convolution_convert_fusion = bf16[1024,2048]{1,0:T(8,128)(2,1)} fusion(bf16[1024,2048]{0,1:T(8,128)(2,1)} %bitcast.17, bf16[1024,2048]{0,1:T(8,128)(2,1)} %fusion.1, bf16[2048,1024]{1,0:T(8,128)(2,1)} %all-gather.5.cloned.1.call-done), kind=kOutput, calls=%fused_computation.6 | convolution fusion | flops 8595177472 | bytes 16777216 | tf_op jit(solution)/shard_map/dot_general | solution.py:20
  232.7 0.0 reduce-scatter.2.cloned.1.call-update
  232.7 6.5 %copy.14 = bf16[1024,2048]{1,0:T(8,128)(2,1)} copy(bf16[1024,2048]{0,1:T(8,128)(2,1)} %bitcast.18) | data formatting | bytes 8388608
  239.2 36.7 %reduce-scatter.2.cloned.1.call-done = bf16[1024,512]{1,0:T(8,128)(2,1)} async-done(((bf16[1024,2048]{1,0:T(8,128)(2,1)}), bf16[1024,512]{1,0:T(8,128)(2,1)}) %reduce-scatter.2.cloned.1.call-update) | async-done | bytes 1048592 | tf_op jit(solution)/shard_map/reduce_scatter | solution.py:21
  275.8 4.6 %copy.16 = bf16[2048,1024]{1,0:T(8,128)(2,1)} copy(bf16[2048,1024]{1,0:T(8,128)(2,1)} %all-gather.5.cloned.1.call-done) | data formatting | bytes 8388608
  (1 shorter events, 0.0 us)
Async XLA Ops:
  7.2 79.1 %all-gather.7.cloned.1.call-start = ((), (), s32[]{:S(2)}) async-start(), calls=%async_computation.3 | async-start | bytes 4718592 | tf_op jit(solution)/shard_map/all_gather | solution.py:11
  9.3 134.1 %all-gather.9.cloned.1.call-start = ((), (), s32[]{:S(2)}) async-start(), calls=%async_computation.5 | async-start | bytes 5242880 | tf_op jit(solution)/shard_map/all_gather | solution.py:13
  10.1 208.3 %all-gather.5.cloned.1.call-start = ((), (), s32[]{:S(2)}) async-start(), calls=%async_computation.2 | async-start | bytes 4718592 | tf_op jit(solution)/shard_map/all_gather | solution.py:9
  86.2 82.4 %all-to-all-start = ((bf16[4,1024,512]{2,1,0:T(8,128)(2,1)}), bf16[4,1024,512]{2,1,0:T(8,128)(2,1)}, u32[]{:S(2)}, u32[]{:S(2)}) async-start(bf16[4,1024,512]{2,1,0:T(8,128)(2,1)} %bitcast.19), calls=%async_computation | async-start | bytes 8388608 | tf_op jit(solution)/shard_map/all_to_all | solution.py:12
  91.2 184.7 %reduce-scatter.2.cloned.1.call-start = ((), (), s32[]{:S(2)}) async-start(), calls=%async_computation.4 | async-start | bytes 5242880 | tf_op jit(solution)/shard_map/reduce_scatter | solution.py:21
Sparse Core Ops, SparseCore 0:
  10.7 75.5 all-gather.6
  87.8 55.5 all-gather.8
  145.5 72.7 all-gather.4
  232.9 42.9 reduce-scatter.1
